TPU v7x, 512 devices: a whole 4x4x16 slice. The times are simulated.
512 devices in a mesh: sp: 64 (over z, y), tp: 8 (over x, core).
Axes of the slice: x: 4, y: 4, z: 16, core: 2. Of those that a mesh axis runs over, the one named last changes fastest.
Arguments:
- tokens: bfloat16 [24576, 2048], P(('sp', 'tp')), may hold values from -6 to 6
- norm_gain: float32 [2048], replicated, may hold values from 0.1 to 1.9
- conv_in_weight: bfloat16 [2048, 2048], P('sp', 'tp'), may hold values from -0.125 to 0.125
- conv_gate_weight: bfloat16 [2048, 2048], P('sp', 'tp'), may hold values from -0.125 to 0.125
- conv_taps: float32 [3, 2048], replicated, may hold values from -3 to 3
- query_weight: bfloat16 [2048, 1024], P('sp', 'tp'), may hold values from -0.125 to 0.125
- key_weight: bfloat16 [2048, 1024], P('sp', 'tp'), may hold values from -0.125 to 0.125
- value_weight: bfloat16 [2048, 2048], P('sp', 'tp'), may hold values from -0.125 to 0.125
- decay_down: bfloat16 [2048, 16], replicated, may hold values from -0.125 to 0.125
- decay_up: bfloat16 [16, 1024], replicated, may hold values from -1.5 to 1.5
- decay_bias: float32 [1024], replicated, may hold values from 0.2 to 10
- decay_extra: float32 [8, 24576], P('tp', 'sp'), may hold values from -2.2 to 0
- head_gain: float32 [2048], replicated, may hold values from 0.1 to 1.9
- conv_out_weight: bfloat16 [2048, 2048], P('tp', 'sp'), may hold values from -0.125 to 0.125
- value_out_weight: bfloat16 [2048, 2048], P('tp', 'sp'), may hold values from -0.125 to 0.125
Outputs:
- mixed: bfloat16 [24576, 2048], P(('sp', 'tp'))
All inputs are finite; a program needn't handle non-finite values.
Results may differ from a plain program's by a relative error of at most 0.02.
Values may be sent and summed in bfloat16 or wider, within the bound.
A program may use at most 64 MiB of HBM per device.

v0:
```python
import math
import jax
import jax.numpy as jnp
from jax import lax
from jax.sharding import Mesh
from jax.sharding import PartitionSpec as P

KEY_DIM = 128
VAL_DIM = 256
BLOCK = 64
SP = ("sp_0", "sp_1")
SP_TP = ("sp_0", "sp_1", "tp")
EPSILON = 1e-06


def nothing_yet(array, identity):
    return jax.tree.map(
        lambda part, zero: jnp.zeros_like(part) + jnp.asarray(zero, part.dtype), array, identity
    )


def prefix_by_axis(array, axes, combine, identity, reverse):
    before = start = nothing_yet(array, identity)
    subtotal = array
    for axis in reversed(axes):
        count, place = (lax.axis_size(axis), lax.axis_index(axis))
        pieces = jax.tree.map(
            lambda part, kind: lax.all_gather(part.astype(kind), axis),
            subtotal,
            (jnp.bfloat16, jnp.bfloat16),
        )
        inside, subtotal = (start, start)
        for k in reversed(range(count)) if reverse else range(count):
            passed = k > place if reverse else k < place
            subtotal = combine(
                subtotal, jax.tree.map(lambda part, own: part[k].astype(own.dtype), pieces, array)
            )
            inside = jax.tree.map(lambda new, old: jnp.where(passed, new, old), subtotal, inside)
        before = combine(inside, before)
    return before


def copy_for_each(array, axis):
    count = lax.axis_size(axis)
    return lax.all_to_all(
        jnp.broadcast_to(array[None], (count, *array.shape)), axis, 0, 0, tiled=True
    )


def joined_along(blocks, dim):
    blocks = jnp.moveaxis(blocks, 0, dim)
    dims = blocks.shape
    return blocks.reshape(*dims[:dim], dims[dim] * dims[dim + 1], *dims[dim + 2 :])


def gathered_copies(array, axis, dim):
    blocks = copy_for_each(array, axis)
    return joined_along(blocks, dim)


def rows_first(arrays, axis, dims):
    turned = [jnp.moveaxis(a, dim, 0) for a, dim in zip(arrays, dims)]
    widths = [t[0].size for t in turned]
    both = jnp.concatenate([t.reshape(-1, w) for t, w in zip(turned, widths)], axis=1)
    filled = lax.all_gather(both, axis, axis=0, tiled=True)
    blocks = jnp.split(filled, [sum(widths[:k]) for k in range(1, len(widths))], axis=1)
    return tuple(
        (
            jnp.moveaxis(b.reshape(-1, *t.shape[1:]), 0, dim)
            for b, t, dim in zip(blocks, turned, dims)
        )
    )


def padded_2(block, sides, width):
    for axis, dim in sides:
        count = lax.axis_size(axis)
        forward = [(i, i + 1) for i in range(count - 1)]
        backward = [(target, source) for source, target in forward]
        low = lax.ppermute(
            lax.slice_in_dim(block, block.shape[dim] - width, None, axis=dim), axis, forward
        )
        high = lax.ppermute(lax.slice_in_dim(block, 0, width, axis=dim), axis, backward)
        block = jnp.concatenate([low, block, high], axis=dim)
    return block


def cut_along(array, dim, count):
    before, after = (array.shape[:dim], array.shape[dim + 1 :])
    return jnp.moveaxis(array.reshape(*before, count, -1, *after), dim, 0)


def sum_at_owner(array, axis, dim):
    blocks = cut_along(array, dim, lax.axis_size(axis))
    arrived = lax.all_to_all(blocks, axis, split_axis=0, concat_axis=0, tiled=True)
    return arrived.astype(jnp.float32).sum(axis=0)


def rms_rows(inputs, scale_gain):
    floats = inputs.astype(jnp.float32)
    return (
        floats * lax.rsqrt(jnp.mean(floats * floats, axis=-1, keepdims=True) + EPSILON) * scale_gain
    )


def rounded(inputs):
    return lax.optimization_barrier(inputs.astype(jnp.bfloat16)).astype(jnp.float32)


def project(normed, weight):
    return jnp.dot(normed, weight, preferred_element_type=jnp.float32)


def chain_combine(earlier, later):
    return (earlier[0] * later[0], later[0][..., None] * earlier[1] + later[1])


def gla_heads(queries, key_rows, values, log_decay):
    length, head_count, key_dim = queries.shape
    val_dim = values.shape[-1]
    blocks = length // BLOCK
    query_float = queries.astype(jnp.float32).reshape(blocks, BLOCK, head_count, key_dim)
    key_float = key_rows.astype(jnp.float32).reshape(blocks, BLOCK, head_count, key_dim)
    value_float = values.astype(jnp.float32).reshape(blocks, BLOCK, head_count, val_dim)
    decay_blocks = log_decay.reshape(blocks, BLOCK, head_count, key_dim)
    cumul = jnp.cumsum(decay_blocks, axis=1)
    before = cumul - decay_blocks
    totals = cumul[:, -1]
    offsets = jnp.cumsum(totals, axis=0) - totals
    whole_decay = jnp.sum(totals, axis=0)
    element_indices = jnp.arange(BLOCK)
    lower_mask = element_indices[:, None] >= element_indices[None, :]
    fwd_query = query_float * jnp.exp(cumul)
    fwd_scores = jnp.einsum("nihd,njhd->nhij", fwd_query, key_float * jnp.exp(-cumul))
    fwd_scores = jnp.where(lower_mask, fwd_scores, 0.0)
    key_start = key_float * jnp.exp(before)
    back_scores = jnp.einsum("nihd,njhd->nhij", query_float * jnp.exp(-before), key_start)
    back_scores = jnp.where(lower_mask.T, back_scores, 0.0)
    within = jnp.einsum("nhij,njhe->nihe", fwd_scores + back_scores, value_float)
    fwd_inc = jnp.einsum(
        "njhd,njhe->nhde", key_float * jnp.exp(totals[:, None] - cumul), value_float
    )
    back_inc = jnp.einsum("njhd,njhe->nhde", key_start, value_float)
    tail_decay = jnp.exp(whole_decay[None] - offsets - totals)
    fwd_device = jnp.einsum("nhd,nhde->hde", tail_decay, fwd_inc)
    back_device = jnp.einsum("nhd,nhde->hde", jnp.exp(offsets), back_inc)
    identity = (jnp.ones_like(whole_decay), jnp.zeros_like(fwd_device))
    incoming_fwd = prefix_by_axis(
        (jnp.exp(whole_decay), fwd_device), SP, chain_combine, identity, False
    )[1]
    incoming_back = prefix_by_axis(
        (jnp.exp(whole_decay), back_device), SP, chain_combine, identity, True
    )[1]
    block_order = jnp.arange(blocks)
    earlier_mask = (block_order[:, None] > block_order[None, :])[:, :, None, None]
    gap_fwd = offsets[:, None] - offsets[None, :] - totals[None, :]
    weights_fwd = jnp.exp(jnp.where(earlier_mask, gap_fwd, -jnp.inf))
    starts_fwd = (
        jnp.einsum("bchd,chde->bhde", weights_fwd, fwd_inc)
        + jnp.exp(offsets)[..., None] * incoming_fwd[None]
    )
    later_mask = (block_order[:, None] < block_order[None, :])[:, :, None, None]
    gap_back = offsets[None, :] - offsets[:, None] - totals[:, None]
    weights_back = jnp.exp(jnp.where(later_mask, gap_back, -jnp.inf))
    next_back = (
        jnp.einsum("bchd,chde->bhde", weights_back, back_inc)
        + tail_decay[..., None] * incoming_back[None]
    )
    carried_terms = jnp.einsum("nihd,nhde->nihe", fwd_query, starts_fwd)
    carried_terms = carried_terms + jnp.einsum(
        "nihd,nhde->nihe", query_float * jnp.exp(totals[:, None] - before), next_back
    )
    return (within + carried_terms).reshape(length, head_count, val_dim)


def local(
    tokens,
    norm_gain,
    conv_in_weight,
    conv_gate_weight,
    conv_taps,
    query_weight,
    key_weight,
    value_weight,
    decay_down,
    decay_up,
    decay_bias,
    decay_extra,
    head_gain,
    conv_out_weight,
    value_out_weight,
):
    shard_index = lax.axis_index("tp")
    channels = conv_in_weight.shape[1]
    key_width = query_weight.shape[1]
    val_width = value_weight.shape[1]
    head_count = decay_extra.shape[0]
    gathered = gathered_copies(tokens, "tp", 0)
    normed = rms_rows(gathered, norm_gain).astype(jnp.bfloat16)
    length = normed.shape[0]
    gathered_weights = rows_first(
        (
            conv_in_weight,
            conv_gate_weight,
            query_weight,
            key_weight,
            value_weight,
            conv_out_weight,
            value_out_weight,
        ),
        SP,
        (0, 0, 0, 0, 0, 1, 1),
    )
    conv_pre = project(normed, gathered_weights[0])
    gate_pre = project(normed, gathered_weights[1])
    probe_before_norm = project(normed, gathered_weights[2])
    key_pre = project(normed, gathered_weights[3])
    value_pre = project(normed, gathered_weights[4])
    conv_out_full = gathered_weights[5]
    value_out_full = gathered_weights[6]
    conv_in = conv_pre.astype(jnp.bfloat16)
    padded = padded_2(conv_in, ((SP, 0),), 1).astype(jnp.float32)
    tap_slice = lax.dynamic_slice_in_dim(conv_taps, shard_index * channels, channels, 1)
    mixed_conv = (
        padded[:-2] * tap_slice[0] + padded[1:-1] * tap_slice[1] + padded[2:] * tap_slice[2]
    )
    conv_mixed = (mixed_conv * jax.nn.silu(rounded(gate_pre))).astype(jnp.bfloat16)
    queries = (probe_before_norm * (1.0 / math.sqrt(KEY_DIM))).astype(jnp.bfloat16)
    key_rows = key_pre.astype(jnp.bfloat16)
    values = value_pre.astype(jnp.bfloat16)
    low_rank = project(normed, decay_down).astype(jnp.bfloat16)
    key_offset = shard_index * key_width
    up_slice = lax.dynamic_slice_in_dim(decay_up, key_offset, key_width, 1)
    bias_slice = lax.dynamic_slice_in_dim(decay_bias, key_offset, key_width, 0)
    log_decay = jax.nn.log_sigmoid(project(low_rank, up_slice) + bias_slice) / 16.0
    log_decay = log_decay.reshape(length, head_count, KEY_DIM) + decay_extra.T[:, :, None]
    raw_mixed = gla_heads(
        queries.reshape(length, head_count, KEY_DIM),
        key_rows.reshape(length, head_count, KEY_DIM),
        values.reshape(length, head_count, VAL_DIM),
        log_decay,
    )
    gain_slice = lax.dynamic_slice_in_dim(head_gain, shard_index * val_width, val_width, 0).reshape(
        head_count, VAL_DIM
    )
    gla_mixed = rms_rows(raw_mixed, gain_slice).astype(jnp.bfloat16).reshape(length, val_width)
    mixed = sum_at_owner(
        (project(conv_mixed, conv_out_full) + project(gla_mixed, value_out_full)).astype(
            jnp.bfloat16
        ),
        "tp",
        0,
    )
    return mixed.astype(jnp.bfloat16)


def solution(mesh):
    torus = Mesh(mesh.devices.reshape(16, 4, mesh.shape["tp"]), ("sp_0", "sp_1", "tp"))
    return jax.shard_map(
        local,
        mesh=torus,
        in_specs=(
            P(SP_TP, None),
            P(),
            P(SP, "tp"),
            P(SP, "tp"),
            P(),
            P(SP, "tp"),
            P(SP, "tp"),
            P(SP, "tp"),
            P(),
            P(),
            P(),
            P("tp", SP),
            P(),
            P("tp", SP),
            P("tp", SP),
        ),
        out_specs=P(SP_TP, None),
        check_vma=False,
    )
```

profile of v0, /device:TPU:1, one launch (start us, length us, event | category | flops | bytes accessed | tf_op | source)
XLA Modules:
  0.0 377.7 jit_solution(13934947043964088281)
XLA Ops:
  6.5 0.8 constant_dynamic-update-slice_fusion.6
  7.3 0.7 constant_dynamic-update-slice_fusion.5
  8.0 0.7 constant_dynamic-update-slice_fusion.4
  8.7 0.7 constant_dynamic-update-slice_fusion.3
  9.4 0.7 constant_dynamic-update-slice_fusion.2
  10.1 0.7 constant_dynamic-update-slice_fusion.1
  10.9 0.7 constant_dynamic-update-slice_fusion
  12.3 2.3 broadcast_in_dim.36
  14.5 10.5 %all-to-all-start = ((bf16[8,48,2048]{2,1,0:T(8,128)(2,1)}), bf16[8,48,2048]{2,1,0:T(8,128)(2,1)S(1)}, u32[]{:S(2)}, u32[]{:S(2)}) async-start(bf16[8,48,2048]{2,1,0:T(8,128)(2,1)} %broadcast_in_dim.36), calls=%async_computation | async-start | bytes 3145728 | tf_op jit(solution)/shard_map/all_to_all | solution.py:45
  25.0 0.8 dynamic_slice.14
  25.8 19.8 %all-to-all-done = bf16[8,48,2048]{2,1,0:T(8,128)(2,1)S(1)} async-done(((bf16[8,48,2048]{2,1,0:T(8,128)(2,1)}), bf16[8,48,2048]{2,1,0:T(8,128)(2,1)S(1)}, u32[]{:S(2)}, u32[]{:S(2)}) %all-to-all-start) | async-done | bytes 1572896 | tf_op jit(solution)/shard_map/all_to_all | solution.py:45
  46.5 1.5 fusion.58
  48.6 5.9 %all-gather.3 = bf16[4,1,128]{2,1,0:T(2,128)(2,1)S(1)} all-gather(bf16[1,1,128]{2,1,0:T(2,128)(2,1)S(1)} %convert_bitcast_fusion), channel_id=2, replica_groups=mesh['sp_0'=16,'sp_1'=4,'tp'=8] {'sp_1'}, dimensions={0}, use_global_device_ids=true | all-gather | bytes 1280 | tf_op jit(solution)/shard_map/all_gather | solution.py:28
  55.1 105.2 %all-gather.8.cloned.1.call-done = bf16[2048,1536]{1,0:T(8,128)(2,1)} async-done(((bf16[32,1536]{1,0:T(8,128)(2,1)}), bf16[2048,1536]{1,0:T(8,128)(2,1)}) %all-gather.8.cloned.1.call-update) | async-done | bytes 6291472 | tf_op jit(solution)/shard_map/all_gather | solution.py:65
  160.4 1.6 convolution_convert_fusion.3
  162.0 1.8 convolution_convert_fusion
  164.5 9.4 %all-gather.2 = bf16[512,256]{1,0:T(8,128)(2,1)S(1)} all-gather(bf16[128,256]{1,0:T(8,128)(2,1)S(1)} %bitcast.364), channel_id=4, replica_groups=mesh['sp_0'=16,'sp_1'=4,'tp'=8] {'sp_1'}, dimensions={0}, use_global_device_ids=true | all-gather | bytes 327680 | tf_op jit(solution)/shard_map/all_gather | solution.py:28
  174.6 10.3 %all-gather.1 = bf16[512,256]{1,0:T(8,128)(2,1)S(1)} all-gather(bf16[128,256]{1,0:T(8,128)(2,1)S(1)} %bitcast.365), channel_id=3, replica_groups=mesh['sp_0'=16,'sp_1'=4,'tp'=8] {'sp_1'}, dimensions={0}, use_global_device_ids=true | all-gather | bytes 327680 | tf_op jit(solution)/shard_map/all_gather | solution.py:28
  184.9 0.8 fusion.87
  185.9 1.3 dynamic_slice.15
  188.3 0.9 constant_dynamic-slice_fusion
  189.2 0.7 copy.40
  189.9 0.7 copy.56
  190.7 0.7 copy.47
  191.4 0.7 copy.43
  192.1 0.7 copy.53
  192.9 20.4 %all_gather.43 = bf16[16,1,128]{2,1,0:T(2,128)(2,1)S(1)} all-gather(bf16[1,1,128]{2,1,0:T(2,128)(2,1)S(1)} %get-tuple-element.51), channel_id=1, replica_groups=mesh['sp_0'=16,'sp_1'=4,'tp'=8] {'sp_0'}, dimensions={0}, use_global_device_ids=true | all-gather | bytes 4352 | tf_op jit(solution)/shard_map/all_gather | solution.py:28
  213.3 19.5 %all_gather.39 = bf16[16,1,128]{2,1,0:T(2,128)(2,1)S(1)} all-gather(bf16[1,1,128]{2,1,0:T(2,128)(2,1)S(1)} %get-tuple-element.52), channel_id=1, replica_groups=mesh['sp_0'=16,'sp_1'=4,'tp'=8] {'sp_0'}, dimensions={0}, use_global_device_ids=true | all-gather | bytes 4352 | tf_op jit(solution)/shard_map/all_gather | solution.py:28
  235.1 1.8 convolution_convert_fusion.2
  236.9 1.9 collective-permute-start
  238.8 1.3 collective-permute-start.1
  240.1 1.6 fusion.8
  241.8 1.8 convolution_convert_fusion.1
  243.6 0.9 convolution_select_fusion.1
  244.5 1.9 fusion.17
  246.5 7.6 %all-gather.10.cloned.1.call-done = bf16[16,1,128,256]{3,2,1,0:T(8,128)(2,1)} async-done(((bf16[1,1,128,256]{3,2,1,0:T(8,128)(2,1)}), bf16[16,1,128,256]{3,2,1,0:T(8,128)(2,1)}) %all-gather.10.cloned.1.call-update) | async-done | bytes 1048592 | tf_op jit(solution)/shard_map/all_gather | solution.py:28
  254.1 2.0 fusion.86
  256.2 1.6 fusion.3
  257.8 1.0 fusion.22
  258.8 65.4 %all-gather.12.cloned.1.call-done = bf16[16,1,128,256]{3,2,1,0:T(8,128)(2,1)} async-done(((bf16[1,1,128,256]{3,2,1,0:T(8,128)(2,1)}), bf16[16,1,128,256]{3,2,1,0:T(8,128)(2,1)}) %all-gather.12.cloned.1.call-update) | async-done | bytes 1048592 | tf_op jit(solution)/shard_map/all_gather | solution.py:28
  324.2 2.0 fusion.79
  326.3 1.7 fusion.5
  328.1 1.0 convolution_add_fusion.1
  329.0 2.5 fusion.42
  331.6 1.1 fusion.41
  332.7 1.8 add_convert_fusion
  334.6 35.6 %all_to_all.10 = bf16[8,48,2048]{2,1,0:T(8,128)(2,1)S(1)} all-to-all(bf16[8,48,2048]{2,1,0:T(8,128)(2,1)S(1)} %bitcast.348), channel_id=1, replica_groups=mesh['sp_0'=16,'sp_1'=4,'tp'=8] {'tp'}, dimensions={0} | all-to-all | bytes 3145728 | tf_op jit(solution)/shard_map/all_to_all | solution.py:95
  370.2 0.9 reduce_sum.42
  (85 shorter events, 7.8 us)
Async XLA Ops:
  6.5 40.0 %copy-start = (bf16[2048,16]{0,1:T(8,128)(2,1)S(1)}, bf16[2048,16]{0,1:T(8,128)(2,1)}, u32[]{:S(2)}) copy-start(bf16[2048,16]{0,1:T(8,128)(2,1)} %param.23) | copy-start | bytes 196612
  6.5 153.8 %all-gather.8.cloned.1.call-start = ((), (), s32[]{:S(2)}) async-start(), calls=%async_computation.2 | async-start | bytes 6389760 | tf_op jit(solution)/shard_map/all_gather | solution.py:65
  11.6 0.7 copy-start.12
  14.5 11.2 %copy-start.20 = (f32[1,384]{1,0:T(1,128)S(1)}, f32[1,384]{1,0:T(1,128)}, u32[]{:S(2)}) copy-start(f32[1,384]{1,0:T(1,128)} %param.26) | copy-start | bytes 4612
  14.5 31.1 %all-to-all-start = ((bf16[8,48,2048]{2,1,0:T(8,128)(2,1)}), bf16[8,48,2048]{2,1,0:T(8,128)(2,1)S(1)}, u32[]{:S(2)}, u32[]{:S(2)}) async-start(bf16[8,48,2048]{2,1,0:T(8,128)(2,1)} %broadcast_in_dim.36), calls=%async_computation | async-start | bytes 3145728 | tf_op jit(solution)/shard_map/all_to_all | solution.py:45
  25.0 21.1 %copy-start.13 = (f32[2048]{0:T(1024)S(1)}, f32[2048]{0:T(1024)}, u32[]{:S(2)}) copy-start(f32[2048]{0:T(1024)} %param.16) | copy-start | bytes 24580
  25.0 229.1 %all-gather.10.cloned.1.call-start = ((), (), s32[]{:S(2)}) async-start(), calls=%async_computation.3 | async-start | bytes 1114112 | tf_op jit(solution)/shard_map/all_gather | solution.py:28
  48.1 115.7 %copy-start.1 = (f32[384,128]{1,0:T(8,128)}, f32[384,128]{1,0:T(8,128)S(1)}, u32[]{:S(2)}) copy-start(f32[384,128]{1,0:T(8,128)S(1)} %fusion.58) | copy-start | bytes 589828
  163.8 10.4 %copy-start.5 = (bf16[384,256]{1,0:T(8,128)(2,1)}, bf16[384,256]{1,0:T(8,128)(2,1)S(1)}, u32[]{:S(2)}) copy-start(bf16[384,256]{1,0:T(8,128)(2,1)S(1)} %convolution_convert_fusion) | copy-start | bytes 589828
  164.1 10.5 %copy-start.11 = (bf16[6,128,256]{2,1,0:T(8,128)(2,1)}, bf16[6,128,256]{2,1,0:T(8,128)(2,1)S(1)}, u32[]{:S(2)}) copy-start(bf16[6,128,256]{2,1,0:T(8,128)(2,1)S(1)} %fusion.89) | copy-start | bytes 1179652
  173.9 11.0 %copy-start.3 = (bf16[512,256]{1,0:T(8,128)(2,1)}, bf16[512,256]{1,0:T(8,128)(2,1)S(1)}, u32[]{:S(2)}) copy-start(bf16[512,256]{1,0:T(8,128)(2,1)S(1)} %all-gather.2) | copy-start | bytes 786436
  174.2 11.6 %copy-start.10 = (bf16[6,128,256]{2,1,0:T(8,128)(2,1)}, bf16[6,128,256]{2,1,0:T(8,128)(2,1)S(1)}, u32[]{:S(2)}) copy-start(bf16[6,128,256]{2,1,0:T(8,128)(2,1)S(1)} %fusion.54) | copy-start | bytes 1179652
  184.9 0.9 copy-start.4
  185.8 138.4 %all-gather.12.cloned.1.call-start = ((), (), s32[]{:S(2)}) async-start(), calls=%async_computation.4 | async-start | bytes 1114112 | tf_op jit(solution)/shard_map/all_gather | solution.py:28
  236.9 7.5 %collective-permute-start = (bf16[1,256]{1,0:T(2,128)(2,1)S(1)}, bf16[1,256]{1,0:T(2,128)(2,1)S(1)}, u32[]{:S(2)}, u32[]{:S(2)}) collective-permute-start(bf16[1,256]{1,0:T(2,128)(2,1)S(1)} %get-tuple-element.10), channel_id=1, source_target_pairs={{0,8},{8,16},{16,24},{24,32},{32,40},{40,48},{48,56},{56,64},{64,7... | collective-permute-start | bytes 1544 | tf_op jit(solution)/shard_map/ppermute | solution.py:80
  238.8 5.7 %collective-permute-start.1 = (bf16[1,256]{1,0:T(2,128)(2,1)S(1)}, bf16[1,256]{1,0:T(2,128)(2,1)S(1)}, u32[]{:S(2)}, u32[]{:S(2)}) collective-permute-start(bf16[1,256]{1,0:T(2,128)(2,1)S(1)} %get-tuple-element.11), channel_id=1, source_target_pairs={{8,0},{16,8},{24,16},{32,24},{40,32},{48,40},{56,48},{64,56},{72,6... | collective-permute-start | bytes 1544 | tf_op jit(solution)/shard_map/ppermute | solution.py:83
  241.7 1.9 copy-start.6
  254.1 3.7 copy-start.7
  256.1 68.1 %copy-start.15 = (f32[128]{0:T(128)S(1)}, f32[128]{0:T(128)}, u32[]{:S(2)}) copy-start(f32[128]{0:T(128)} %get-tuple-element.47) | copy-start | bytes 1540
  256.1 68.1 %copy-start.16 = (f32[128]{0:T(128)S(1)}, f32[128]{0:T(128)}, u32[]{:S(2)}) copy-start(f32[128]{0:T(128)} %get-tuple-element.15) | copy-start | bytes 1540
  256.1 68.1 %copy-start.17 = (f32[128]{0:T(128)S(1)}, f32[128]{0:T(128)}, u32[]{:S(2)}) copy-start(f32[128]{0:T(128)} %get-tuple-element.16) | copy-start | bytes 1540
  256.1 68.1 %copy-start.18 = (f32[128]{0:T(128)S(1)}, f32[128]{0:T(128)}, u32[]{:S(2)}) copy-start(f32[128]{0:T(128)} %get-tuple-element.17) | copy-start | bytes 1540
  256.2 68.1 %copy-start.19 = (f32[128]{0:T(128)S(1)}, f32[128]{0:T(128)}, u32[]{:S(2)}) copy-start(f32[128]{0:T(128)} %get-tuple-element.18) | copy-start | bytes 1540
  326.3 1.8 copy-start.2
  326.3 1.8 copy-start.8
  326.3 1.8 copy-start.9
  328.0 3.6 copy-start.14
Sparse Core Ops, SparseCore 0:
  12.4 147.9 all-gather.7
  185.9 68.0 all-gather.9
  256.2 67.9 all-gather.11
where the time goes:
time: 379 us; the launch traced here: 378 us
  waiting for transfers between devices  198 us (52%)
  blocking collectives  101 us (27%)
  matrix products  24 us (6%)
  local copies, waits for them, and re-layouts  15.1 us (4%)
  starting transfers between devices  13.7 us (4%)
  between operations  13.6 us (4%)
  other arithmetic  12.1 us (3%)
    all_gather x1, waiting for transfers between devices, rows_first(): filled = lax.all_gather(both, axis, axis=0, tiled=True)  105 us
    all_gather x2, waiting for transfers between devices, prefix_by_axis(): lax.all_gather(part.astype(kind), axis)  73 us
    all_gather x5, blocking collectives, prefix_by_axis(): lax.all_gather(part.astype(kind), axis)  65.4 us
    all_to_all x1, blocking collectives, sum_at_owner(): lax.all_to_all(blocks, axis, split_axis=0, concat_axis=0, tiled=True)  35.6 us
    all_to_all x1, waiting for transfers between devices, copy_for_each(): lax.all_to_all(jnp.broadcast_to(array[None], (count, *array.shape)), axis...  19.8 us
    dot_general x8, matrix products, project(): return jnp.dot(normed, weight, preferred_element_type=jnp.float32)  14 us
    all_to_all x1, starting transfers between devices, copy_for_each(): lax.all_to_all(jnp.broadcast_to(array[None], (count, *array.shape)), axis...  10.5 us
  transfers between devices with their start and end apart: 6, of which 4 were waited for; matrix products, arithmetic and copies ran while one was open for 8% of the time, Pallas kernels for 0%

commit v1 on v0

--- a/solution.py
+++ b/solution.py
@@ -62,7 +62,10 @@
     turned = [jnp.moveaxis(a, dim, 0) for a, dim in zip(arrays, dims)]
     widths = [t[0].size for t in turned]
     both = jnp.concatenate([t.reshape(-1, w) for t, w in zip(turned, widths)], axis=1)
-    filled = lax.all_gather(both, axis, axis=0, tiled=True)
+    filled = jnp.concatenate(
+        jax.lax.all_to_all(jnp.stack([both for _ in range(jax.lax.axis_size(axis))]), axis, 0, 0),
+        axis=0,
+    )
     blocks = jnp.split(filled, [sum(widths[:k]) for k in range(1, len(widths))], axis=1)
     return tuple(
         (

time: 379 us -> 543 us (1.43)
  waiting for transfers between devices: 198 us -> 340 us
  starting transfers between devices: 13.7 us -> 30.1 us
  blocking collectives: 101 us -> 109 us
    all_to_all x0 -> x1, waiting for transfers between devices: none -> 259 us  [rows_first(): jax.lax.all_to_all(jnp.stack([both for _ in range(jax.lax.axis_size(axis)...]
    all_gather x1 -> x0, waiting for transfers between devices: 105 us -> none  [rows_first(): filled = lax.all_gather(both, axis, axis=0, tiled=True)]
    all_to_all x0 -> x1, starting transfers between devices: none -> 14.3 us  [rows_first(): jax.lax.all_to_all(jnp.stack([both for _ in range(jax.lax.axis_size(axis)...]
    all_gather x2, waiting for transfers between devices: 73 us -> 60.1 us  [prefix_by_axis(): lax.all_gather(part.astype(kind), axis)]
    all_gather x5, blocking collectives: 65.4 us -> 72.9 us  [prefix_by_axis(): lax.all_gather(part.astype(kind), axis)]
  transfers between devices with their start and end apart: 6 -> 6, of which waited for: 4 -> 3; matrix products, arithmetic and copies ran while one was open for 8% -> 5% of each run, Pallas kernels for 0% -> 0%
where the time goes in v1:
time: 543 us; the launch traced here: 542 us
  waiting for transfers between devices  340 us (63%)
  blocking collectives  109 us (20%)
  starting transfers between devices  30.1 us (6%)
  matrix products  24 us (4%)
  between operations  14.1 us (3%)
  local copies, waits for them, and re-layouts  13 us (2%)
  other arithmetic  12.3 us (2%)
    all_to_all x1, waiting for transfers between devices, rows_first(): jax.lax.all_to_all(jnp.stack([both for _ in range(jax.lax.axis_size(axis)...  259 us
    all_gather x5, blocking collectives, prefix_by_axis(): lax.all_gather(part.astype(kind), axis)  72.9 us
    all_gather x2, waiting for transfers between devices, prefix_by_axis(): lax.all_gather(part.astype(kind), axis)  60.1 us
    all_to_all x1, blocking collectives, sum_at_owner(): lax.all_to_all(blocks, axis, split_axis=0, concat_axis=0, tiled=True)  35.7 us
    all_to_all x1, waiting for transfers between devices, copy_for_each(): lax.all_to_all(jnp.broadcast_to(array[None], (count, *array.shape)), axis...  20.5 us
    all_to_all x1, starting transfers between devices, rows_first(): jax.lax.all_to_all(jnp.stack([both for _ in range(jax.lax.axis_size(axis)...  14.3 us
    dot_general x8, matrix products, project(): return jnp.dot(normed, weight, preferred_element_type=jnp.float32)  14 us
  transfers between devices with their start and end apart: 6, of which 3 were waited for; matrix products, arithmetic and copies ran while one was open for 5% of the time, Pallas kernels for 0%

profile of v1, /device:TPU:1, one launch (start us, length us, event | category | flops | bytes accessed | tf_op | source)
XLA Modules:
  0.0 541.6 jit_solution(2652016022174196841)
XLA Ops:
  6.6 2.4 broadcast_in_dim.36
  9.0 10.3 %all-to-all-start = ((bf16[8,48,2048]{2,1,0:T(8,128)(2,1)}), bf16[8,48,2048]{2,1,0:T(8,128)(2,1)S(1)}, u32[]{:S(2)}, u32[]{:S(2)}) async-start(bf16[8,48,2048]{2,1,0:T(8,128)(2,1)} %broadcast_in_dim.36), calls=%async_computation | async-start | bytes 3145728 | tf_op jit(solution)/shard_map/all_to_all | solution.py:45
  19.4 20.5 %all-to-all-done = bf16[8,48,2048]{2,1,0:T(8,128)(2,1)S(1)} async-done(((bf16[8,48,2048]{2,1,0:T(8,128)(2,1)}), bf16[8,48,2048]{2,1,0:T(8,128)(2,1)S(1)}, u32[]{:S(2)}, u32[]{:S(2)}) %all-to-all-start) | async-done | bytes 1572896 | tf_op jit(solution)/shard_map/all_to_all | solution.py:45
  39.9 3.4 stack.2
  43.3 14.3 %all-to-all-start.1 = ((bf16[64,32,1536]{2,1,0:T(8,128)(2,1)}), bf16[64,32,1536]{2,1,0:T(8,128)(2,1)}, u32[]{:S(2)}, u32[]{:S(2)}) async-start(bf16[64,32,1536]{2,1,0:T(8,128)(2,1)} %stack.2), calls=%async_computation.1 | async-start | bytes 12582912 | tf_op jit(solution)/shard_map/all_to_all | solution.py:66
  57.7 0.8 dynamic_slice.14
  58.5 1.3 dynamic_slice.15
  60.7 1.5 fusion.58
  62.8 8.2 %all-gather.3 = bf16[4,1,128]{2,1,0:T(2,128)(2,1)S(1)} all-gather(bf16[1,1,128]{2,1,0:T(2,128)(2,1)S(1)} %convert_bitcast_fusion), channel_id=2, replica_groups=mesh['sp_0'=16,'sp_1'=4,'tp'=8] {'sp_1'}, dimensions={0}, use_global_device_ids=true | all-gather | bytes 1280 | tf_op jit(solution)/shard_map/all_gather | solution.py:28
  71.0 0.6 broadcast_select_fusion.3
  71.6 258.9 %all-to-all-done.1 = bf16[64,32,1536]{2,1,0:T(8,128)(2,1)} async-done(((bf16[64,32,1536]{2,1,0:T(8,128)(2,1)}), bf16[64,32,1536]{2,1,0:T(8,128)(2,1)}, u32[]{:S(2)}, u32[]{:S(2)}) %all-to-all-start.1) | async-done | bytes 6291488 | tf_op jit(solution)/shard_map/all_to_all | solution.py:66
  330.5 1.8 convolution_convert_fusion
  332.3 1.7 convolution_convert_fusion.3
  335.1 9.4 %all-gather.2 = bf16[512,256]{1,0:T(8,128)(2,1)S(1)} all-gather(bf16[128,256]{1,0:T(8,128)(2,1)S(1)} %bitcast.365), channel_id=4, replica_groups=mesh['sp_0'=16,'sp_1'=4,'tp'=8] {'sp_1'}, dimensions={0}, use_global_device_ids=true | all-gather | bytes 327680 | tf_op jit(solution)/shard_map/all_gather | solution.py:28
  344.8 10.1 %all-gather.1 = bf16[512,256]{1,0:T(8,128)(2,1)S(1)} all-gather(bf16[128,256]{1,0:T(8,128)(2,1)S(1)} %bitcast.366), channel_id=3, replica_groups=mesh['sp_0'=16,'sp_1'=4,'tp'=8] {'sp_1'}, dimensions={0}, use_global_device_ids=true | all-gather | bytes 327680 | tf_op jit(solution)/shard_map/all_gather | solution.py:28
  355.0 0.8 fusion.87
  355.9 0.6 iota_compare_fusion.3
  356.5 0.6 iota_compare_fusion.2
  357.1 0.9 constant_dynamic-slice_fusion
  358.0 0.7 copy.56
  358.7 0.7 copy.40
  359.4 0.7 copy.47
  360.2 0.7 copy.43
  360.9 0.7 copy.53
  361.6 25.3 %all_gather.35 = bf16[16,1,128]{2,1,0:T(2,128)(2,1)S(1)} all-gather(bf16[1,1,128]{2,1,0:T(2,128)(2,1)S(1)} %get-tuple-element.52), channel_id=1, replica_groups=mesh['sp_0'=16,'sp_1'=4,'tp'=8] {'sp_0'}, dimensions={0}, use_global_device_ids=true | all-gather | bytes 4352 | tf_op jit(solution)/shard_map/all_gather | solution.py:28
  386.9 19.9 %all_gather.39 = bf16[16,1,128]{2,1,0:T(2,128)(2,1)S(1)} all-gather(bf16[1,1,128]{2,1,0:T(2,128)(2,1)S(1)} %get-tuple-element.51), channel_id=1, replica_groups=mesh['sp_0'=16,'sp_1'=4,'tp'=8] {'sp_0'}, dimensions={0}, use_global_device_ids=true | all-gather | bytes 4352 | tf_op jit(solution)/shard_map/all_gather | solution.py:28
  406.8 0.6 fusion.115
  407.9 0.7 fusion.130
  408.6 0.7 fusion.113
  409.2 1.8 convolution_convert_fusion.2
  411.1 1.3 collective-permute-start.1
  412.4 4.2 collective-permute-start
  416.5 1.6 fusion.8
  418.2 1.8 convolution_convert_fusion.1
  420.0 0.9 convolution_select_fusion.1
  420.9 1.9 fusion.17
  423.0 2.1 fusion.86
  425.0 1.6 fusion.3
  426.7 1.0 fusion.22
  427.6 60.1 %all-gather.9.cloned.1.call-done = bf16[16,1,128,256]{3,2,1,0:T(8,128)(2,1)} async-done(((bf16[1,1,128,256]{3,2,1,0:T(8,128)(2,1)}), bf16[16,1,128,256]{3,2,1,0:T(8,128)(2,1)}) %all-gather.9.cloned.1.call-update) | async-done | bytes 1048592 | tf_op jit(solution)/shard_map/all_gather | solution.py:28
  487.7 2.1 fusion.79
  489.9 1.7 fusion.5
  491.6 1.0 convolution_add_fusion.1
  492.6 2.5 fusion.42
  495.1 1.1 fusion.41
  496.2 1.8 add_convert_fusion
  498.1 35.7 %all_to_all.15 = bf16[8,48,2048]{2,1,0:T(8,128)(2,1)S(1)} all-to-all(bf16[8,48,2048]{2,1,0:T(8,128)(2,1)S(1)} %bitcast.349), channel_id=1, replica_groups=mesh['sp_0'=16,'sp_1'=4,'tp'=8] {'tp'}, dimensions={0} | all-to-all | bytes 3145728 | tf_op jit(solution)/shard_map/all_to_all | solution.py:98
  533.8 0.9 reduce_sum.42
  (95 shorter events, 3.8 us)
Async XLA Ops:
  6.5 54.2 %copy-start = (bf16[2048,16]{0,1:T(8,128)(2,1)S(1)}, bf16[2048,16]{0,1:T(8,128)(2,1)}, u32[]{:S(2)}) copy-start(bf16[2048,16]{0,1:T(8,128)(2,1)} %param.23) | copy-start | bytes 196612
  6.5 12.8 %copy-start.12 = (bf16[32,256]{1,0:T(8,128)(2,1)S(1)}, bf16[32,256]{1,0:T(8,128)(2,1)}, u32[]{:S(2)}) copy-start(bf16[32,256]{1,0:T(8,128)(2,1)} %param.17) | copy-start | bytes 49156
  6.5 12.8 %copy-start.13 = (bf16[32,256]{1,0:T(8,128)(2,1)S(1)}, bf16[32,256]{1,0:T(8,128)(2,1)}, u32[]{:S(2)}) copy-start(bf16[32,256]{1,0:T(8,128)(2,1)} %param.18) | copy-start | bytes 49156
  6.5 12.8 %copy-start.18 = (bf16[32,128]{1,0:T(8,128)(2,1)S(1)}, bf16[32,128]{1,0:T(8,128)(2,1)}, u32[]{:S(2)}) copy-start(bf16[32,128]{1,0:T(8,128)(2,1)} %param.20) | copy-start | bytes 24580
  6.5 12.8 %copy-start.19 = (bf16[32,128]{1,0:T(8,128)(2,1)S(1)}, bf16[32,128]{1,0:T(8,128)(2,1)}, u32[]{:S(2)}) copy-start(bf16[32,128]{1,0:T(8,128)(2,1)} %param.21) | copy-start | bytes 24580
  6.5 12.8 %copy-start.14 = (bf16[32,256]{1,0:T(8,128)(2,1)S(1)}, bf16[32,256]{1,0:T(8,128)(2,1)}, u32[]{:S(2)}) copy-start(bf16[32,256]{1,0:T(8,128)(2,1)} %param.22) | copy-start | bytes 49156
  6.6 12.8 %copy-start.15 = (bf16[256,32]{0,1:T(8,128)(2,1)S(1)}, bf16[256,32]{0,1:T(8,128)(2,1)}, u32[]{:S(2)}) copy-start(bf16[256,32]{0,1:T(8,128)(2,1)} %param.28) | copy-start | bytes 49156
  6.6 12.8 %copy-start.16 = (bf16[256,32]{0,1:T(8,128)(2,1)S(1)}, bf16[256,32]{0,1:T(8,128)(2,1)}, u32[]{:S(2)}) copy-start(bf16[256,32]{0,1:T(8,128)(2,1)} %param.29) | copy-start | bytes 49156
  9.0 30.9 %all-to-all-start = ((bf16[8,48,2048]{2,1,0:T(8,128)(2,1)}), bf16[8,48,2048]{2,1,0:T(8,128)(2,1)S(1)}, u32[]{:S(2)}, u32[]{:S(2)}) async-start(bf16[8,48,2048]{2,1,0:T(8,128)(2,1)} %broadcast_in_dim.36), calls=%async_computation | async-start | bytes 3145728 | tf_op jit(solution)/shard_map/all_to_all | solution.py:45
  43.3 14.4 %copy-start.24 = (f32[1,384]{1,0:T(1,128)S(1)}, f32[1,384]{1,0:T(1,128)}, u32[]{:S(2)}) copy-start(f32[1,384]{1,0:T(1,128)} %param.26) | copy-start | bytes 4612
  43.3 17.0 %copy-start.17 = (f32[2048]{0:T(1024)S(1)}, f32[2048]{0:T(1024)}, u32[]{:S(2)}) copy-start(f32[2048]{0:T(1024)} %param.16) | copy-start | bytes 24580
  43.3 287.2 %all-to-all-start.1 = ((bf16[64,32,1536]{2,1,0:T(8,128)(2,1)}), bf16[64,32,1536]{2,1,0:T(8,128)(2,1)}, u32[]{:S(2)}, u32[]{:S(2)}) async-start(bf16[64,32,1536]{2,1,0:T(8,128)(2,1)} %stack.2), calls=%async_computation.1 | async-start | bytes 12582912 | tf_op jit(solution)/shard_map/all_to_all | solution.py:66
  57.5 365.4 %all-gather.7.cloned.1.call-start = ((), (), s32[]{:S(2)}) async-start(), calls=%async_computation.3 | async-start | bytes 1114112 | tf_op jit(solution)/shard_map/all_gather | solution.py:28
  62.3 272.1 %copy-start.1 = (f32[384,128]{1,0:T(8,128)}, f32[384,128]{1,0:T(8,128)S(1)}, u32[]{:S(2)}) copy-start(f32[384,128]{1,0:T(8,128)S(1)} %fusion.58) | copy-start | bytes 589828
  332.3 2.8 copy-start.5
  334.3 76.7 %copy-start.10 = (bf16[6,128,256]{2,1,0:T(8,128)(2,1)}, bf16[6,128,256]{2,1,0:T(8,128)(2,1)S(1)}, u32[]{:S(2)}) copy-start(bf16[6,128,256]{2,1,0:T(8,128)(2,1)S(1)} %fusion.54) | copy-start | bytes 1179652
  334.7 76.4 %copy-start.11 = (bf16[6,128,256]{2,1,0:T(8,128)(2,1)}, bf16[6,128,256]{2,1,0:T(8,128)(2,1)S(1)}, u32[]{:S(2)}) copy-start(bf16[6,128,256]{2,1,0:T(8,128)(2,1)S(1)} %fusion.89) | copy-start | bytes 1179652
  344.5 10.5 %copy-start.3 = (bf16[512,256]{1,0:T(8,128)(2,1)}, bf16[512,256]{1,0:T(8,128)(2,1)S(1)}, u32[]{:S(2)}) copy-start(bf16[512,256]{1,0:T(8,128)(2,1)S(1)} %all-gather.2) | copy-start | bytes 786436
  355.0 0.8 copy-start.4
  355.9 131.8 %all-gather.9.cloned.1.call-start = ((), (), s32[]{:S(2)}) async-start(), calls=%async_computation.4 | async-start | bytes 1114112 | tf_op jit(solution)/shard_map/all_gather | solution.py:28
  411.1 9.8 %collective-permute-start.1 = (bf16[1,256]{1,0:T(2,128)(2,1)S(1)}, bf16[1,256]{1,0:T(2,128)(2,1)S(1)}, u32[]{:S(2)}, u32[]{:S(2)}) collective-permute-start(bf16[1,256]{1,0:T(2,128)(2,1)S(1)} %get-tuple-element.11), channel_id=1, source_target_pairs={{8,0},{16,8},{24,16},{32,24},{40,32},{48,40},{56,48},{64,56},{72,6... | collective-permute-start | bytes 1544 | tf_op jit(solution)/shard_map/ppermute | solution.py:86
  412.4 8.5 %collective-permute-start = (bf16[1,256]{1,0:T(2,128)(2,1)S(1)}, bf16[1,256]{1,0:T(2,128)(2,1)S(1)}, u32[]{:S(2)}, u32[]{:S(2)}) collective-permute-start(bf16[1,256]{1,0:T(2,128)(2,1)S(1)} %get-tuple-element.10), channel_id=1, source_target_pairs={{0,8},{8,16},{16,24},{24,32},{32,40},{40,48},{48,56},{56,64},{64,7... | collective-permute-start | bytes 1544 | tf_op jit(solution)/shard_map/ppermute | solution.py:83
  418.2 2.8 copy-start.6
  422.9 64.8 %copy-start.21 = (f32[128]{0:T(128)S(1)}, f32[128]{0:T(128)}, u32[]{:S(2)}) copy-start(f32[128]{0:T(128)} %get-tuple-element.47) | copy-start | bytes 1540
  422.9 64.8 %copy-start.22 = (f32[128]{0:T(128)S(1)}, f32[128]{0:T(128)}, u32[]{:S(2)}) copy-start(f32[128]{0:T(128)} %get-tuple-element.15) | copy-start | bytes 1540
  422.9 64.8 %copy-start.23 = (f32[128]{0:T(128)S(1)}, f32[128]{0:T(128)}, u32[]{:S(2)}) copy-start(f32[128]{0:T(128)} %get-tuple-element.16) | copy-start | bytes 1540
  422.9 3.7 copy-start.7
  425.0 64.9 %copy-start.25 = (pred[6,6]{1,0:T(8,128)(4,1)S(1)}, pred[6,6]{1,0:T(8,128)(4,1)}, u32[]{:S(2)}) copy-start(pred[6,6]{1,0:T(8,128)(4,1)} %iota_compare_fusion.2) | copy-start | bytes 112
  487.7 3.9 copy-start.2
  487.7 3.9 copy-start.8
  487.7 3.9 copy-start.9
  489.9 5.2 copy-start.20
Sparse Core Ops, SparseCore 0:
  356.0 61.7 all-gather.6
  419.9 67.7 all-gather.8
